TPU v7x, 512 devices: a whole 4x4x16 slice. The times are simulated.
512 devices in a mesh: ep: 32 (over z, core), tp: 16 (over y, x).
Axes of the slice: x: 4, y: 4, z: 16, core: 2. Of those that a mesh axis runs over, the one named last changes fastest.
Arguments:
- conv_input: bfloat16 [1024, 65536], P('tp', 'ep'), may hold values from -6 to 6
- out_gate: bfloat16 [1024, 65536], P('tp', 'ep'), may hold values from -6 to 6
- in_gate: bfloat16 [1024, 65536], P('tp', 'ep'), may hold values from -6 to 6
- conv_taps: float32 [3, 1024], replicated, may hold values from -3.5 to 3.5
- mixer_proj: bfloat16 [1024, 2048], P(None, 'tp'), may hold values from -0.1875 to 0.1875
- token_rows: bfloat16 [8192, 2048], P('ep', 'tp'), may hold values from -4000 to 4000
- routes: int32 [8192, 2], P('ep'), may hold values from 0 to 31, as said below
- route_weights: float32 [8192, 2], P('ep'), may hold values from 0.3 to 1
- expert_gate: bfloat16 [32, 2048, 4096], P('ep', None, 'tp'), may hold values from -0.125 to 0.125
- expert_up: bfloat16 [32, 2048, 4096], P('ep', None, 'tp'), may hold values from -0.125 to 0.125
- expert_down: bfloat16 [32, 4096, 2048], P('ep', 'tp'), may hold values from -0.125 to 0.125
Outputs:
- mixed_out: bfloat16 [65536, 2048], P('ep', 'tp')
- expert_out: bfloat16 [8192, 2048], P('ep', 'tp')
Inputs may be any that keep to these rules, and one draw needn't show every extreme that they name: `routes`: in each aligned block of 256 rows, no expert is named more than 32 times and one expert, the same in every block, exactly 32 times; the two experts of a row differ.
All inputs are finite; a program needn't handle non-finite values.
Results may differ from a plain program's by a relative error of at most 0.015.
Values may be sent and summed in bfloat16 or wider, within the bound.
A program may use at most 64 MiB of HBM per device.

v0:
```python
import jax
import jax.numpy as jnp
from jax import lax
from jax.sharding import PartitionSpec as P

KERNEL = 3
EPSILON = 1e-06


def passed_along(value, axis, by):
    devices = lax.axis_size(axis)
    pairs = [(i, i + by) for i in range(devices) if 0 <= i + by < devices]
    return lax.ppermute(value, axis, pairs)


def split_up(value, dim, devices):
    before, after = (value.shape[:dim], value.shape[dim + 1 :])
    return jnp.moveaxis(value.reshape(*before, devices, -1, *after), dim, 0)


def sent_and_summed(value, axis, dim):
    blocks = split_up(value, dim, lax.axis_size(axis))
    arrived = lax.all_to_all(blocks, axis, split_axis=0, concat_axis=0, tiled=True)
    return arrived.astype(jnp.float32).sum(axis=0)


def slot_places(route_ids, capacity, experts):
    flat_ids = route_ids.reshape(-1)
    hit_table = (flat_ids[:, None] == jnp.arange(experts, dtype=jnp.int32)[None, :]).astype(
        jnp.int32
    )
    earlier = jnp.cumsum(hit_table, axis=0) - hit_table
    slot_rank = jnp.sum(earlier * hit_table, axis=1)
    return flat_ids * capacity + slot_rank


def body(
    conv_input,
    out_gate,
    in_gate,
    conv_taps,
    mixer_proj,
    token_rows,
    routes,
    route_weights,
    expert_gate,
    expert_up,
    expert_down,
):
    width_part = conv_input.shape[0]
    length = conv_input.shape[1]
    offset = lax.axis_index("tp") * width_part
    local_taps = lax.dynamic_slice_in_dim(conv_taps, offset, width_part, 1)
    z_rows = (conv_input.astype(jnp.float32) * in_gate.astype(jnp.float32)).astype(jnp.bfloat16)
    rim_rows = passed_along(z_rows[:, length - (KERNEL - 1) :], "ep", 1)
    longer = jnp.concatenate([rim_rows, z_rows], axis=1).astype(jnp.float32)
    conv_sum = jnp.zeros(z_rows.shape, jnp.float32)
    for lag_index in range(KERNEL):
        begin = KERNEL - 1 - lag_index
        conv_sum = conv_sum + local_taps[lag_index][:, None] * longer[:, begin : begin + length]
    gated = (out_gate.astype(jnp.float32) * conv_sum).astype(jnp.bfloat16)
    mixed_sum = lax.dot_general(
        lax.all_gather(gated, "tp", axis=0, tiled=True),
        mixer_proj,
        (((0,), (0,)), ((), ())),
        preferred_element_type=jnp.float32,
    )
    mixed_out = mixed_sum.astype(jnp.bfloat16)
    experts = lax.axis_size("ep")
    rows_b = token_rows.shape[0]
    cols_part = token_rows.shape[1]
    capacity = 4 * rows_b // experts
    slot_total = experts * capacity
    places = slot_places(routes, capacity, experts)
    sources = jnp.arange(2 * rows_b, dtype=jnp.int32) // 2
    gate_weight = expert_gate[0]
    up_weight = expert_up[0]
    down_weight = expert_down[0]
    feature_count = cols_part * lax.axis_size("tp")
    buffer = jnp.zeros((slot_total, cols_part), jnp.bfloat16).at[places].set(token_rows[sources])
    arrived = lax.all_to_all(
        buffer.reshape(experts, capacity, cols_part), "ep", split_axis=0, concat_axis=0, tiled=True
    )
    arrived = arrived.reshape(slot_total, cols_part)
    part_in = lax.all_gather(arrived, "tp", axis=1, tiled=True)
    gate_sum = jnp.dot(part_in, gate_weight, preferred_element_type=jnp.float32)
    up_sum = jnp.dot(part_in, up_weight, preferred_element_type=jnp.float32)
    squares = jnp.sum(jnp.square(part_in.astype(jnp.float32)), axis=1)
    row_scale = lax.rsqrt(squares / feature_count + EPSILON)[:, None]
    hidden = (jax.nn.silu(row_scale * gate_sum) * (row_scale * up_sum)).astype(jnp.bfloat16)
    summed = sent_and_summed(
        lax.dot_general(
            down_weight, hidden, (((0,), (1,)), ((), ())), preferred_element_type=jnp.float32
        ).astype(jnp.bfloat16),
        "tp",
        0,
    )
    expert_rows = summed.astype(jnp.bfloat16).reshape(cols_part, experts, capacity)
    returned = lax.all_to_all(expert_rows, "ep", split_axis=1, concat_axis=1, tiled=True).reshape(
        cols_part, slot_total
    )
    picked = returned[:, places].astype(jnp.float32).reshape(cols_part, rows_b, 2)
    combined = jnp.sum(picked * route_weights[None, :, :], axis=2)
    expert_out = combined.T.astype(jnp.bfloat16)
    return (mixed_out, expert_out)


def solution(mesh):
    return jax.shard_map(
        body,
        mesh=mesh,
        in_specs=(
            P("tp", "ep"),
            P("tp", "ep"),
            P("tp", "ep"),
            P(),
            P(None, "tp"),
            P("ep", "tp"),
            P("ep", None),
            P("ep", None),
            P("ep", None, "tp"),
            P("ep", None, "tp"),
            P("ep", "tp", None),
        ),
        out_specs=(P("ep", "tp"), P("ep", "tp")),
        check_vma=False,
    )
```

profile of v0, /device:TPU:1, one launch (start us, length us, event | category | flops | bytes accessed | tf_op | source)
XLA Modules:
  0.0 242.8 jit_solution(143505425020026601)
XLA Ops:
  7.2 0.0 copy-start
  7.2 0.0 all-gather.5.cloned.1.call-start
  7.2 0.9 copy.26
  8.1 0.1 eq.29
  8.3 0.1 eq.25
  8.4 0.7 broadcast_multiply_fusion
  9.1 1.2 reduce-window.6
  10.3 0.2 slice_reduce_fusion
  10.6 0.1 copy.25
  10.7 0.1 mul.101
  10.9 0.1 fusion.18
  11.0 4.9 %scatter_custom_fusion = bf16[1024,128]{1,0:T(8,128)(2,1)S(1)} fusion(s32[512]{0:T(512)S(1)} %bitcast.65, bf16[256,128]{1,0:T(8,128)(2,1)} %param.16, s32[1024]{0:T(1024)S(1)} %pad_clamp_fusion.1, bf16[]{:T(256)} %constant.39.clone.1), kind=kCustom, calls=%fused_computation.26 | custom fusion | bytes 262656 | tf_op jit(solution)/shard_map/scatter | solution.py:80
  15.9 38.9 %all_to_all.15 = bf16[32,32,128]{2,1,0:T(8,128)(2,1)} all-to-all(bf16[32,32,128]{2,1,0:T(8,128)(2,1)S(1)} %bitcast.63), channel_id=1, replica_groups=mesh['ep'=32,'tp'=16] {'ep'}, dimensions={0} | all-to-all | bytes 524288 | tf_op jit(solution)/shard_map/all_to_all | solution.py:81
  54.8 0.0 copy-start.3
  54.8 0.0 all-gather.5.cloned.1.call-update
  54.8 0.0 all-gather.3.cloned.1.call-start
  54.9 1.2 multiply_convert_fusion
  56.0 0.1 slice.40
  56.1 2.2 collective-permute-start
  58.4 0.8 constant_dynamic-slice_fusion
  59.1 0.1 collective-permute-done
  59.2 0.1 maximum_convert_fusion
  59.4 2.0 fusion.9
  61.4 0.0 all-gather.3.cloned.1.call-update
  61.4 55.6 %all-gather.5.cloned.1.call-done = bf16[1024,2048]{1,0:T(8,128)(2,1)} async-done(((bf16[1024,128]{1,0:T(8,128)(2,1)}), bf16[1024,2048]{1,0:T(8,128)(2,1)}) %all-gather.5.cloned.1.call-update) | async-done | bytes 4194320 | tf_op jit(solution)/shard_map/all_gather | solution.py:85
  117.1 0.0 copy-start.1
  117.1 3.2 %multiply_reduce_fusion = f32[1024]{0:T(1024)S(1)} fusion(bf16[1024,2048]{1,0:T(8,128)(2,1)} %all-gather.5.cloned.1.call-done), kind=kLoop, calls=%fused_computation.3 | loop fusion | flops 6290432 | bytes 4198400 | tf_op jit(solution)/shard_map/reduce_sum | solution.py:88
  120.3 0.0 copy-start.4
  120.3 0.0 copy-done.3
  120.3 0.2 copy-done.1
  120.5 2.3 convolution_multiply_fusion.1
  122.8 0.0 copy-done
  122.8 0.0 copy-done.4
  122.8 8.8 %convert_bitcast_fusion = bf16[128,16,8,128]{3,2,1,0:T(8,128)(2,1)} fusion(bf16[1,256,2048]{2,1,0:T(8,128)(2,1)S(1)} %copy-done, bf16[1024,2048]{1,0:T(8,128)(2,1)} %all-gather.5.cloned.1.call-done, bf16[1,2048,256]{2,1,0:T(8,128)(2,1)S(1)} %copy-done.4, f32[1024,256]{1,0:T(8,128)} %convolution_multiply_fusion.1, f32[1024]{0:T(1024)S(1)} %add_rsqrt_fusion), kind=kOutput, calls=%fused_computation.5 | convolution fusion | flops 2151415808 | bytes 11538432 | tf_op jit(solution)/shard_map/dot_general | solution.py:92
  131.6 3.3 %copy.35 = bf16[128,16,8,128]{3,2,0,1:T(8,128)(2,1)S(1)} copy(bf16[128,16,8,128]{3,2,1,0:T(8,128)(2,1)} %convert_bitcast_fusion) | data formatting | bytes 8388608 | tf_op jit(solution)/shard_map/reshape | solution.py:18
  134.9 58.8 %all_to_all.16 = bf16[16,128,1024]{1,2,0:T(8,128)(2,1)} all-to-all(bf16[16,128,1024]{1,2,0:T(8,128)(2,1)S(1)} %bitcast.59), channel_id=1, replica_groups=mesh['ep'=32,'tp'=16] {'tp'}, dimensions={0} | all-to-all | bytes 8388608 | tf_op jit(solution)/shard_map/all_to_all | solution.py:23
  193.7 0.0 copy-start.2
  193.7 0.0 copy-start.5
  193.7 3.9 %reduce_sum.44 = bf16[128,1024]{0,1:T(8,128)(2,1)} reduce(bf16[16,128,1024]{1,2,0:T(8,128)(2,1)} %all_to_all.16, bf16[]{:T(256)} %constant.39.clone.1), dimensions={0}, to_apply=%region_5.6 | reduce | flops 1966080 | bytes 4456450 | tf_op jit(solution)/shard_map/reduce_sum | solution.py:24
  197.6 13.7 %all-to-all-start.2 = ((bf16[128,32,32]{0,2,1:T(8,128)(2,1)}), bf16[128,32,32]{0,2,1:T(8,128)(2,1)S(1)}, u32[]{:S(2)}, u32[]{:S(2)}) async-start(bf16[128,32,32]{0,2,1:T(8,128)(2,1)} %bitcast.13), calls=%async_computation.2 | async-start | bytes 524288 | tf_op jit(solution)/shard_map/all_to_all | solution.py:99
  211.3 0.0 copy-done.2
  211.3 0.1 copy.30
  211.5 3.2 %all-gather.3.cloned.1.call-done = bf16[1024,2048]{1,0:T(8,128)(2,1)} async-done(((bf16[64,2048]{1,0:T(8,128)(2,1)}), bf16[1024,2048]{1,0:T(8,128)(2,1)}) %all-gather.3.cloned.1.call-update) | async-done | bytes 4194320 | tf_op jit(solution)/shard_map/all_gather | solution.py:63
  214.7 0.0 copy-done.5
  214.7 4.3 %convolution_convert_fusion = bf16[2048,128]{1,0:T(8,128)(2,1)} fusion(bf16[1024,2048]{1,0:T(8,128)(2,1)} %all-gather.3.cloned.1.call-done, bf16[1024,128]{1,0:T(8,128)(2,1)S(1)} %copy-done.5), kind=kOutput, calls=%fused_computation.6 | convolution fusion | flops 537133056 | bytes 4980736 | tf_op jit(solution)/shard_map/dot_general | solution.py:62
  219.0 14.6 %all-to-all-done.2 = bf16[128,32,32]{0,2,1:T(8,128)(2,1)S(1)} async-done(((bf16[128,32,32]{0,2,1:T(8,128)(2,1)}), bf16[128,32,32]{0,2,1:T(8,128)(2,1)S(1)}, u32[]{:S(2)}, u32[]{:S(2)}) %all-to-all-start.2) | async-done | bytes 262176 | tf_op jit(solution)/shard_map/all_to_all | solution.py:99
  233.6 1.3 gather_fusion
  234.9 1.0 multiply_reduce_fusion.1
  (10 shorter events, 0.1 us)
Async XLA Ops:
  7.2 115.7 %copy-start = (bf16[1,256,2048]{2,1,0:T(8,128)(2,1)S(1)}, bf16[1,256,2048]{2,1,0:T(8,128)(2,1)}, u32[]{:S(2)}) copy-start(bf16[1,256,2048]{2,1,0:T(8,128)(2,1)} %param.21) | copy-start | bytes 3145732
  7.2 109.9 %all-gather.5.cloned.1.call-start = ((), (), s32[]{:S(2)}) async-start(), calls=%async_computation.4 | async-start | bytes 4456448 | tf_op jit(solution)/shard_map/all_gather | solution.py:85
  54.8 65.5 %copy-start.3 = (bf16[1,2048,256]{2,1,0:T(8,128)(2,1)S(1)}, bf16[1,2048,256]{2,1,0:T(8,128)(2,1)}, u32[]{:S(2)}) copy-start(bf16[1,2048,256]{2,1,0:T(8,128)(2,1)} %param.19) | copy-start | bytes 3145732
  54.8 159.8 %all-gather.3.cloned.1.call-start = ((), (), s32[]{:S(2)}) async-start(), calls=%async_computation.3 | async-start | bytes 4456448 | tf_op jit(solution)/shard_map/all_gather | solution.py:63
  56.1 3.1 %collective-permute-start = (bf16[64,2]{1,0:T(8,128)(2,1)S(1)}, bf16[64,2]{1,0:T(8,128)(2,1)S(1)}, u32[]{:S(2)}, u32[]{:S(2)}) collective-permute-start(bf16[64,2]{1,0:T(8,128)(2,1)S(1)} %slice.40), channel_id=1, source_target_pairs={{0,16},{16,32},{32,48},{48,64},{64,80},{80,96},{96,112},{112,128},... | collective-permute-start | bytes 776 | tf_op jit(solution)/shard_map/ppermute | solution.py:13
  117.1 3.4 %copy-start.1 = (bf16[1024,2048]{1,0:T(8,128)(2,1)S(1)}, bf16[1024,2048]{1,0:T(8,128)(2,1)}, u32[]{:S(2)}) copy-start(bf16[1024,2048]{1,0:T(8,128)(2,1)} %all-gather.5.cloned.1.call-done) | copy-start | bytes 12582916
  120.3 2.5 %copy-start.4 = (bf16[1,2048,256]{2,1,0:T(8,128)(2,1)S(1)}, bf16[1,2048,256]{2,1,0:T(8,128)(2,1)}, u32[]{:S(2)}) copy-start(bf16[1,2048,256]{2,1,0:T(8,128)(2,1)} %param.20) | copy-start | bytes 3145732
  193.7 17.6 %copy-start.2 = (f32[256,2]{0,1:T(2,128)S(1)}, f32[256,2]{0,1:T(2,128)}, u32[]{:S(2)}) copy-start(f32[256,2]{0,1:T(2,128)} %param.18) | copy-start | bytes 6148
  193.7 21.0 %copy-start.5 = (bf16[1024,128]{1,0:T(8,128)(2,1)S(1)}, bf16[1024,128]{1,0:T(8,128)(2,1)}, u32[]{:S(2)}) copy-start(bf16[1024,128]{1,0:T(8,128)(2,1)} %param.15) | copy-start | bytes 786436
  197.6 35.9 %all-to-all-start.2 = ((bf16[128,32,32]{0,2,1:T(8,128)(2,1)}), bf16[128,32,32]{0,2,1:T(8,128)(2,1)S(1)}, u32[]{:S(2)}, u32[]{:S(2)}) async-start(bf16[128,32,32]{0,2,1:T(8,128)(2,1)} %bitcast.13), calls=%async_computation.2 | async-start | bytes 524288 | tf_op jit(solution)/shard_map/all_to_all | solution.py:99
Sparse Core Ops, SparseCore 0:
  54.9 62.0 all-gather.4
  120.6 93.9 all-gather.2
where the time goes:
time: 243 us
  blocking collectives  97.7 us (40%)
  waiting for transfers between devices  73.6 us (30%)
  starting transfers between devices  16 us (7%)
  matrix products  15.4 us (6%)
  between operations  14.2 us (6%)
  other arithmetic  13.6 us (6%)
  local copies, waits for them, and re-layouts  12.4 us (5%)
    all_to_all x1, blocking collectives, sent_and_summed(): lax.all_to_all(blocks, axis, split_axis=0, concat_axis=0, tiled=True)  58.8 us
    all_gather x1, waiting for transfers between devices, body(): part_in = lax.all_gather(arrived, 'tp', axis=1, tiled=True)  55.6 us
    all_to_all x1, blocking collectives, body(): lax.all_to_all(buffer.reshape(experts, capacity, cols_part), 'ep', split_...  38.9 us
    all_to_all x1, waiting for transfers between devices, body(): lax.all_to_all(expert_rows, 'ep', split_axis=1, concat_axis=1, tiled=True)  14.6 us
    all_to_all x1, starting transfers between devices, body(): lax.all_to_all(expert_rows, 'ep', split_axis=1, concat_axis=1, tiled=True)  13.7 us
    dot_general x1, matrix products, body(): lax.dot_general(down_weight, hidden, (((0,), (1,)), ((), ())), preferred_...  8.82 us
    scatter x1, local copies, waits for them, and re-layouts, body(): jnp.zeros((slot_total, cols_part), jnp.bfloat16).at[places]  4.9 us
  transfers between devices with their start and end apart: 4, of which 4 were waited for; matrix products, arithmetic and copies ran while one was open for 12% of the time, Pallas kernels for 0%

commit v1 on v0

--- a/solution.py
+++ b/solution.py
@@ -5,6 +5,12 @@
 
 KERNEL = 3
 EPSILON = 1e-06
+
+
+def reach_modes(piece_in, out_dim):
+    passed = list(piece_in.shape[1:])
+    passed[out_dim] *= piece_in.shape[0]
+    return jnp.moveaxis(piece_in, 0, out_dim).reshape(passed)
 
 
 def passed_along(value, axis, by):
@@ -82,7 +88,24 @@
         buffer.reshape(experts, capacity, cols_part), "ep", split_axis=0, concat_axis=0, tiled=True
     )
     arrived = arrived.reshape(slot_total, cols_part)
-    part_in = lax.all_gather(arrived, "tp", axis=1, tiled=True)
+    chips = lax.axis_size("tp")
+    trail = []
+    for k in range(chips):
+        trail.append((k, (k + 1) % chips))
+    stack_in = []
+    for no, hop_no in trail:
+        stack_in.append((hop_no, no))
+    lower, d_next = ([], [])
+    for nth in range(chips - 1):
+        if nth % 2 == 0:
+            found_now = lax.ppermute(lower[-1] if lower else arrived, "tp", trail)
+            lower.append(found_now)
+        else:
+            d_next.append(lax.ppermute(d_next[-1] if d_next else arrived, "tp", stack_in))
+    block_next = jnp.stack([*lower[::-1], arrived, *d_next])
+    next_value = lax.axis_index("tp") - len(lower)
+    block_next = block_next[(jnp.arange(chips) - next_value) % chips]
+    part_in = reach_modes(block_next, 1)
     gate_sum = jnp.dot(part_in, gate_weight, preferred_element_type=jnp.float32)
     up_sum = jnp.dot(part_in, up_weight, preferred_element_type=jnp.float32)
     squares = jnp.sum(jnp.square(part_in.astype(jnp.float32)), axis=1)

time: 243 us -> 305 us (1.26)
  starting transfers between devices: 16 us -> 84.6 us
  waiting for transfers between devices: 73.6 us -> 38.8 us
  local copies, waits for them, and re-layouts: 12.4 us -> 41.5 us
    ppermute x0 -> x15, starting transfers between devices: none -> 65.3 us  [the longest x7 48.8 us: body(): lax.ppermute(d_next[-1] if d_next else arrived, 'tp', stack_in)]
    all_gather x1 -> x0, waiting for transfers between devices: 55.6 us -> none  [body(): part_in = lax.all_gather(arrived, 'tp', axis=1, tiled=True)]
    ppermute x0 -> x15, waiting for transfers between devices: none -> 21 us  [the longest x8 16.8 us: body(): found_now = lax.ppermute(lower[-1] if lower else arrived, 'tp', trail)]
    unnamed x14 -> x29, local copies, waits for them, and re-layouts: 1.24 us -> 17.7 us
    transpose x0 -> x1, local copies, waits for them, and re-layouts: none -> 6.53 us  [reach_modes(): return jnp.moveaxis(piece_in, 0, out_dim).reshape(passed)]
    gather x0 -> x1, local copies, waits for them, and re-layouts: none -> 5.27 us  [body(): block_next = block_next[(jnp.arange(chips) - next_value) % chips]]
    all_gather x1, waiting for transfers between devices: 3.18 us -> 0.02 us  [body(): lax.all_gather(gated, 'tp', axis=0, tiled=True)]
    all_to_all x1, waiting for transfers between devices: 14.6 us -> 17.8 us  [body(): lax.all_to_all(expert_rows, 'ep', split_axis=1, concat_axis=1, tiled=True)]
  transfers between devices with their start and end apart: 4 -> 18, of which waited for: 4 -> 7; matrix products, arithmetic and copies ran while one was open for 12% -> 19% of each run, Pallas kernels for 0% -> 0%
where the time goes in v1:
time: 305 us; the launch traced here: 304 us
  blocking collectives  95.6 us (31%)
  starting transfers between devices  84.6 us (28%)
  local copies, waits for them, and re-layouts  41.5 us (14%)
  waiting for transfers between devices  38.8 us (13%)
  matrix products  15.5 us (5%)
  between operations  14.4 us (5%)
  other arithmetic  13.2 us (4%)
    all_to_all x1, blocking collectives, sent_and_summed(): lax.all_to_all(blocks, axis, split_axis=0, concat_axis=0, tiled=True)  56.9 us
    ppermute x7, starting transfers between devices, body(): lax.ppermute(d_next[-1] if d_next else arrived, 'tp', stack_in)  48.8 us
    all_to_all x1, blocking collectives, body(): lax.all_to_all(buffer.reshape(experts, capacity, cols_part), 'ep', split_...  38.8 us
    all_to_all x1, waiting for transfers between devices, body(): lax.all_to_all(expert_rows, 'ep', split_axis=1, concat_axis=1, tiled=True)  17.8 us
    unnamed x29, local copies, waits for them, and re-layouts  17.7 us
    ppermute x8, waiting for transfers between devices, body(): found_now = lax.ppermute(lower[-1] if lower else arrived, 'tp', trail)  16.8 us
    ppermute x8, starting transfers between devices, body(): found_now = lax.ppermute(lower[-1] if lower else arrived, 'tp', trail)  16.5 us
    all_to_all x1, starting transfers between devices, body(): lax.all_to_all(expert_rows, 'ep', split_axis=1, concat_axis=1, tiled=True)  14.9 us
  transfers between devices with their start and end apart: 18, of which 7 were waited for; matrix products, arithmetic and copies ran while one was open for 19% of the time, Pallas kernels for 0%

profile of v1, /device:TPU:1, one launch (start us, length us, event | category | flops | bytes accessed | tf_op | source)
XLA Modules:
  0.0 303.7 jit_solution(5204877694375823772)
XLA Ops:
  7.2 0.9 copy.26
  8.1 0.1 eq.31
  8.4 0.7 broadcast_multiply_fusion
  9.1 1.2 reduce-window.6
  10.3 0.2 slice_reduce_fusion
  10.6 0.1 copy.25
  10.7 0.1 mul.101
  11.0 4.9 %scatter_custom_fusion = bf16[1024,128]{1,0:T(8,128)(2,1)S(1)} fusion(s32[512]{0:T(512)S(1)} %bitcast.108, bf16[256,128]{1,0:T(8,128)(2,1)} %param.16, s32[1024]{0:T(1024)S(1)} %pad_clamp_fusion.2, bf16[]{:T(256)} %constant.55.clone.1), kind=kCustom, calls=%fused_computation.43 | custom fusion | bytes 262656 | tf_op jit(solution)/shard_map/scatter | solution.py:86
  15.9 38.8 %all_to_all.15 = bf16[32,32,128]{2,1,0:T(8,128)(2,1)S(1)} all-to-all(bf16[32,32,128]{2,1,0:T(8,128)(2,1)S(1)} %bitcast.106), channel_id=1, replica_groups=mesh['ep'=32,'tp'=16] {'ep'}, dimensions={0} | all-to-all | bytes 524288 | tf_op jit(solution)/shard_map/all_to_all | solution.py:87
  54.7 3.1 %collective-permute-start.1 = (bf16[1024,128]{1,0:T(8,128)(2,1)S(1)}, bf16[1024,128]{1,0:T(8,128)(2,1)S(1)}, u32[]{:S(2)}, u32[]{:S(2)}) collective-permute-start(bf16[1024,128]{1,0:T(8,128)(2,1)S(1)} %bitcast.103), channel_id=1, source_target_pairs={{0,1},{1,2},{2,3},{3,4},{4,5},{5,6},{6,7},{7,8},{8,9},{9,10},{10,1... | collective-permute-start | bytes 786440 | tf_op jit(solution)/shard_map/ppermute | solution.py:101
  57.8 9.6 %collective-permute-done.1 = bf16[1024,128]{1,0:T(8,128)(2,1)S(1)} collective-permute-done((bf16[1024,128]{1,0:T(8,128)(2,1)S(1)}, bf16[1024,128]{1,0:T(8,128)(2,1)S(1)}, u32[]{:S(2)}, u32[]{:S(2)}) %collective-permute-start.1) | collective-permute-done | bytes 262176 | tf_op jit(solution)/shard_map/ppermute | solution.py:101
  67.4 1.9 collective-permute-start.2
  69.3 6.7 %collective-permute-start.9 = (bf16[1024,128]{1,0:T(8,128)(2,1)S(1)}, bf16[1024,128]{1,0:T(8,128)(2,1)S(1)}, u32[]{:S(2)}, u32[]{:S(2)}) collective-permute-start(bf16[1024,128]{1,0:T(8,128)(2,1)S(1)} %bitcast.104), channel_id=1, source_target_pairs={{1,0},{2,1},{3,2},{4,3},{5,4},{6,5},{7,6},{8,7},{9,8},{10,9},{11,1... | collective-permute-start | bytes 786440 | tf_op jit(solution)/shard_map/ppermute | solution.py:104
  76.0 3.1 %collective-permute-done.2 = bf16[1024,128]{1,0:T(8,128)(2,1)S(1)} collective-permute-done((bf16[1024,128]{1,0:T(8,128)(2,1)S(1)}, bf16[1024,128]{1,0:T(8,128)(2,1)S(1)}, u32[]{:S(2)}, u32[]{:S(2)}) %collective-permute-start.2) | collective-permute-done | bytes 262176 | tf_op jit(solution)/shard_map/ppermute | solution.py:101
  79.1 1.9 collective-permute-start.3
  81.0 6.7 %collective-permute-start.10 = (bf16[1024,128]{1,0:T(8,128)(2,1)S(1)}, bf16[1024,128]{1,0:T(8,128)(2,1)S(1)}, u32[]{:S(2)}, u32[]{:S(2)}) collective-permute-start(bf16[1024,128]{1,0:T(8,128)(2,1)S(1)} %collective-permute-done.9), channel_id=1, source_target_pairs={{1,0},{2,1},{3,2},{4,3},{5,4},{6,5},{7,6},{8,7},{9,8},{10,9},{11,1... | collective-permute-start | bytes 786440 | tf_op jit(solution)/shard_map/ppermute | solution.py:104
  87.7 2.2 collective-permute-done.3
  90.0 1.9 collective-permute-start.4
  91.9 6.7 %collective-permute-start.11 = (bf16[1024,128]{1,0:T(8,128)(2,1)S(1)}, bf16[1024,128]{1,0:T(8,128)(2,1)S(1)}, u32[]{:S(2)}, u32[]{:S(2)}) collective-permute-start(bf16[1024,128]{1,0:T(8,128)(2,1)S(1)} %collective-permute-done.10), channel_id=1, source_target_pairs={{1,0},{2,1},{3,2},{4,3},{5,4},{6,5},{7,6},{8,7},{9,8},{10,9},{11,1... | collective-permute-start | bytes 786440 | tf_op jit(solution)/shard_map/ppermute | solution.py:104
  98.6 1.8 collective-permute-done.4
  100.4 1.9 collective-permute-start.5
  102.3 1.1 multiply_convert_fusion
  103.5 4.3 %collective-permute-start = (bf16[64,2]{1,0:T(8,128)(2,1)S(1)}, bf16[64,2]{1,0:T(8,128)(2,1)S(1)}, u32[]{:S(2)}, u32[]{:S(2)}) collective-permute-start(bf16[64,2]{1,0:T(8,128)(2,1)S(1)} %slice.42), channel_id=1, source_target_pairs={{0,16},{16,32},{32,48},{48,64},{64,80},{80,96},{96,112},{112,128},... | collective-permute-start | bytes 776 | tf_op jit(solution)/shard_map/ppermute | solution.py:19
  107.8 0.8 constant_dynamic-slice_fusion
  108.6 7.0 %collective-permute-start.12 = (bf16[1024,128]{1,0:T(8,128)(2,1)S(1)}, bf16[1024,128]{1,0:T(8,128)(2,1)}, u32[]{:S(2)}, u32[]{:S(2)}) collective-permute-start(bf16[1024,128]{1,0:T(8,128)(2,1)S(1)} %collective-permute-done.11), channel_id=1, source_target_pairs={{1,0},{2,1},{3,2},{4,3},{5,4},{6,5},{7,6},{8,7},{9,8},{10,9},{11,1... | collective-permute-start | bytes 786440 | tf_op jit(solution)/shard_map/ppermute | solution.py:104
  115.5 1.9 collective-permute-start.6
  117.5 2.5 collective-permute-done.12
  120.0 7.5 %collective-permute-start.13 = (bf16[1024,128]{1,0:T(8,128)(2,1)}, bf16[1024,128]{1,0:T(8,128)(2,1)}, u32[]{:S(2)}, u32[]{:S(2)}) collective-permute-start(bf16[1024,128]{1,0:T(8,128)(2,1)} %collective-permute-done.12), channel_id=1, source_target_pairs={{1,0},{2,1},{3,2},{4,3},{5,4},{6,5},{7,6},{8,7},{9,8},{10,9},{11,1... | collective-permute-start | bytes 786440 | tf_op jit(solution)/shard_map/ppermute | solution.py:104
  127.5 1.9 collective-permute-start.7
  129.6 1.8 collective-permute-done.13
  131.4 7.4 %collective-permute-start.14 = (bf16[1024,128]{1,0:T(8,128)(2,1)}, bf16[1024,128]{1,0:T(8,128)(2,1)S(1)}, u32[]{:S(2)}, u32[]{:S(2)}) collective-permute-start(bf16[1024,128]{1,0:T(8,128)(2,1)} %collective-permute-done.13), channel_id=1, source_target_pairs={{1,0},{2,1},{3,2},{4,3},{5,4},{6,5},{7,6},{8,7},{9,8},{10,9},{11,1... | collective-permute-start | bytes 786440 | tf_op jit(solution)/shard_map/ppermute | solution.py:104
  138.8 1.9 collective-permute-start.8
  140.8 2.0 fusion.9
  142.8 6.9 %collective-permute-start.15 = (bf16[1024,128]{1,0:T(8,128)(2,1)S(1)}, bf16[1024,128]{1,0:T(8,128)(2,1)S(1)}, u32[]{:S(2)}, u32[]{:S(2)}) collective-permute-start(bf16[1024,128]{1,0:T(8,128)(2,1)S(1)} %collective-permute-done.14), channel_id=1, source_target_pairs={{1,0},{2,1},{3,2},{4,3},{5,4},{6,5},{7,6},{8,7},{9,8},{10,9},{11,1... | collective-permute-start | bytes 786440 | tf_op jit(solution)/shard_map/ppermute | solution.py:104
  149.7 1.7 bitcast_dynamic-update-slice_fusion.15
  151.4 1.7 bitcast_dynamic-update-slice_fusion.14
  153.1 1.7 bitcast_dynamic-update-slice_fusion.13
  154.7 1.7 bitcast_dynamic-update-slice_fusion.12
  156.4 0.7 bitcast_dynamic-update-slice_fusion.11
  157.1 0.7 bitcast_dynamic-update-slice_fusion.10
  157.9 0.7 bitcast_dynamic-update-slice_fusion.9
  158.6 0.7 bitcast_dynamic-update-slice_fusion.8
  159.3 0.7 bitcast_dynamic-update-slice_fusion.7
  160.0 0.7 bitcast_dynamic-update-slice_fusion.6
  160.7 0.7 bitcast_dynamic-update-slice_fusion.5
  161.4 0.7 bitcast_dynamic-update-slice_fusion.4
  162.2 1.7 bitcast_dynamic-update-slice_fusion.3
  163.8 1.7 bitcast_dynamic-update-slice_fusion.2
  165.5 0.7 bitcast_dynamic-update-slice_fusion.1
  166.2 0.8 bitcast_dynamic-update-slice_fusion
  167.0 5.3 %gather_fusion = bf16[16,1024,128]{2,1,0:T(8,128)(2,1)} fusion(bf16[16,1024,128]{2,1,0:T(8,128)(2,1)} %bitcast_dynamic-update-slice_fusion, s32[1024]{0:T(1024)S(1)} %pad_clamp_fusion.1), kind=kCustom, calls=%fused_computation.1 | custom fusion | bytes 8388672 | tf_op jit(solution)/shard_map/gather | solution.py:107
  172.3 6.5 %copy.29 = bf16[1024,16,128]{0,2,1:T(8,128)(2,1)} copy(bf16[1024,16,128]{2,0,1:T(8,128)(2,1)} %bitcast.97) | data formatting | bytes 8388608 | tf_op jit(solution)/shard_map/transpose | solution.py:13
  178.8 3.2 %multiply_reduce_fusion = f32[1024]{0:T(1024)S(1)} fusion(bf16[16,1024,128]{2,1,0:T(8,128)(2,1)} %gather_fusion), kind=kLoop, calls=%fused_computation.4 | loop fusion | flops 6290432 | bytes 4198400 | tf_op jit(solution)/shard_map/reduce_sum | solution.py:111
  182.0 0.2 copy-done.1
  182.3 2.4 convolution_multiply_fusion.1
  184.6 8.8 %convert_bitcast_fusion = bf16[128,16,8,128]{3,2,1,0:T(8,128)(2,1)} fusion(bf16[1,256,2048]{2,1,0:T(8,128)(2,1)S(1)} %copy-done, bf16[1024,2048]{0,1:T(8,128)(2,1)} %bitcast.100, bf16[1,2048,256]{2,1,0:T(8,128)(2,1)S(1)} %copy-done.4, f32[1024,256]{1,0:T(8,128)} %convolution_multiply_fusion.1, f32[1024]{0:T(1024)S(1)} %add_rsqrt_fusion), kind=kOutput, calls=%fused_computation.6 | convolution fusion | flops 2151415808 | bytes 11538432 | tf_op jit(solution)/shard_map/dot_general | solution.py:115
  193.4 3.4 %copy.36 = bf16[128,16,8,128]{3,2,0,1:T(8,128)(2,1)S(1)} copy(bf16[128,16,8,128]{3,2,1,0:T(8,128)(2,1)} %convert_bitcast_fusion) | data formatting | bytes 8388608 | tf_op jit(solution)/shard_map/reshape | solution.py:24
  196.8 56.9 %all_to_all.16 = bf16[16,128,1024]{1,2,0:T(8,128)(2,1)} all-to-all(bf16[16,128,1024]{1,2,0:T(8,128)(2,1)S(1)} %bitcast.98), channel_id=1, replica_groups=mesh['ep'=32,'tp'=16] {'tp'}, dimensions={0} | all-to-all | bytes 8388608 | tf_op jit(solution)/shard_map/all_to_all | solution.py:29
  253.7 3.6 %reduce_sum.44 = bf16[128,1024]{0,1:T(8,128)(2,1)} reduce(bf16[16,128,1024]{1,2,0:T(8,128)(2,1)} %all_to_all.16, bf16[]{:T(256)} %constant.55.clone.1), dimensions={0}, to_apply=%region_5.6 | reduce | flops 1966080 | bytes 4456450 | tf_op jit(solution)/shard_map/reduce_sum | solution.py:30
  257.3 14.9 %all-to-all-start.2 = ((bf16[128,32,32]{0,2,1:T(8,128)(2,1)}), bf16[128,32,32]{0,2,1:T(8,128)(2,1)S(1)}, u32[]{:S(2)}, u32[]{:S(2)}) async-start(bf16[128,32,32]{0,2,1:T(8,128)(2,1)} %bitcast.32), calls=%async_computation.2 | async-start | bytes 524288 | tf_op jit(solution)/shard_map/all_to_all | solution.py:122
  272.4 4.3 %convolution_convert_fusion = bf16[2048,128]{1,0:T(8,128)(2,1)} fusion(bf16[1024,2048]{1,0:T(8,128)(2,1)} %all-gather.2.cloned.1.call-done, bf16[1024,128]{1,0:T(8,128)(2,1)S(1)} %copy-done.5), kind=kOutput, calls=%fused_computation.7 | convolution fusion | flops 537133056 | bytes 4980736 | tf_op jit(solution)/shard_map/dot_general | solution.py:68
  276.7 17.8 %all-to-all-done.2 = bf16[128,32,32]{0,2,1:T(8,128)(2,1)S(1)} async-done(((bf16[128,32,32]{0,2,1:T(8,128)(2,1)}), bf16[128,32,32]{0,2,1:T(8,128)(2,1)S(1)}, u32[]{:S(2)}, u32[]{:S(2)}) %all-to-all-start.2) | async-done | bytes 262176 | tf_op jit(solution)/shard_map/all_to_all | solution.py:122
  294.5 1.3 gather_fusion.1
  295.8 1.0 multiply_reduce_fusion.1
  (41 shorter events, 0.8 us)
Async XLA Ops:
  7.2 177.4 %copy-start = (bf16[1,256,2048]{2,1,0:T(8,128)(2,1)S(1)}, bf16[1,256,2048]{2,1,0:T(8,128)(2,1)}, u32[]{:S(2)}) copy-start(bf16[1,256,2048]{2,1,0:T(8,128)(2,1)} %param.21) | copy-start | bytes 3145732
  7.2 265.2 %all-gather.2.cloned.1.call-start = ((), (), s32[]{:S(2)}) async-start(), calls=%async_computation.3 | async-start | bytes 4456448 | tf_op jit(solution)/shard_map/all_gather | solution.py:69
  54.7 12.7 %collective-permute-start.1 = (bf16[1024,128]{1,0:T(8,128)(2,1)S(1)}, bf16[1024,128]{1,0:T(8,128)(2,1)S(1)}, u32[]{:S(2)}, u32[]{:S(2)}) collective-permute-start(bf16[1024,128]{1,0:T(8,128)(2,1)S(1)} %bitcast.103), channel_id=1, source_target_pairs={{0,1},{1,2},{2,3},{3,4},{4,5},{5,6},{6,7},{7,8},{8,9},{9,10},{10,1... | collective-permute-start | bytes 786440 | tf_op jit(solution)/shard_map/ppermute | solution.py:101
  67.4 11.7 %collective-permute-start.2 = (bf16[1024,128]{1,0:T(8,128)(2,1)S(1)}, bf16[1024,128]{1,0:T(8,128)(2,1)S(1)}, u32[]{:S(2)}, u32[]{:S(2)}) collective-permute-start(bf16[1024,128]{1,0:T(8,128)(2,1)S(1)} %collective-permute-done.1), channel_id=1, source_target_pairs={{0,1},{1,2},{2,3},{3,4},{4,5},{5,6},{6,7},{7,8},{8,9},{9,10},{10,1... | collective-permute-start | bytes 786440 | tf_op jit(solution)/shard_map/ppermute | solution.py:101
  69.3 11.7 %collective-permute-start.9 = (bf16[1024,128]{1,0:T(8,128)(2,1)S(1)}, bf16[1024,128]{1,0:T(8,128)(2,1)S(1)}, u32[]{:S(2)}, u32[]{:S(2)}) collective-permute-start(bf16[1024,128]{1,0:T(8,128)(2,1)S(1)} %bitcast.104), channel_id=1, source_target_pairs={{1,0},{2,1},{3,2},{4,3},{5,4},{6,5},{7,6},{8,7},{9,8},{10,9},{11,1... | collective-permute-start | bytes 786440 | tf_op jit(solution)/shard_map/ppermute | solution.py:104
  79.1 10.9 %collective-permute-start.3 = (bf16[1024,128]{1,0:T(8,128)(2,1)S(1)}, bf16[1024,128]{1,0:T(8,128)(2,1)S(1)}, u32[]{:S(2)}, u32[]{:S(2)}) collective-permute-start(bf16[1024,128]{1,0:T(8,128)(2,1)S(1)} %collective-permute-done.2), channel_id=1, source_target_pairs={{0,1},{1,2},{2,3},{3,4},{4,5},{5,6},{6,7},{7,8},{8,9},{9,10},{10,1... | collective-permute-start | bytes 786440 | tf_op jit(solution)/shard_map/ppermute | solution.py:101
  81.0 10.8 %collective-permute-start.10 = (bf16[1024,128]{1,0:T(8,128)(2,1)S(1)}, bf16[1024,128]{1,0:T(8,128)(2,1)S(1)}, u32[]{:S(2)}, u32[]{:S(2)}) collective-permute-start(bf16[1024,128]{1,0:T(8,128)(2,1)S(1)} %collective-permute-done.9), channel_id=1, source_target_pairs={{1,0},{2,1},{3,2},{4,3},{5,4},{6,5},{7,6},{8,7},{9,8},{10,9},{11,1... | collective-permute-start | bytes 786440 | tf_op jit(solution)/shard_map/ppermute | solution.py:104
  90.0 10.4 %collective-permute-start.4 = (bf16[1024,128]{1,0:T(8,128)(2,1)S(1)}, bf16[1024,128]{1,0:T(8,128)(2,1)S(1)}, u32[]{:S(2)}, u32[]{:S(2)}) collective-permute-start(bf16[1024,128]{1,0:T(8,128)(2,1)S(1)} %collective-permute-done.3), channel_id=1, source_target_pairs={{0,1},{1,2},{2,3},{3,4},{4,5},{5,6},{6,7},{7,8},{8,9},{9,10},{10,1... | collective-permute-start | bytes 786440 | tf_op jit(solution)/shard_map/ppermute | solution.py:101
  91.9 16.7 %collective-permute-start.11 = (bf16[1024,128]{1,0:T(8,128)(2,1)S(1)}, bf16[1024,128]{1,0:T(8,128)(2,1)S(1)}, u32[]{:S(2)}, u32[]{:S(2)}) collective-permute-start(bf16[1024,128]{1,0:T(8,128)(2,1)S(1)} %collective-permute-done.10), channel_id=1, source_target_pairs={{1,0},{2,1},{3,2},{4,3},{5,4},{6,5},{7,6},{8,7},{9,8},{10,9},{11,1... | collective-permute-start | bytes 786440 | tf_op jit(solution)/shard_map/ppermute | solution.py:104
  100.4 15.1 %collective-permute-start.5 = (bf16[1024,128]{1,0:T(8,128)(2,1)S(1)}, bf16[1024,128]{1,0:T(8,128)(2,1)}, u32[]{:S(2)}, u32[]{:S(2)}) collective-permute-start(bf16[1024,128]{1,0:T(8,128)(2,1)S(1)} %collective-permute-done.4), channel_id=1, source_target_pairs={{0,1},{1,2},{2,3},{3,4},{4,5},{5,6},{6,7},{7,8},{8,9},{9,10},{10,1... | collective-permute-start | bytes 786440 | tf_op jit(solution)/shard_map/ppermute | solution.py:101
  103.5 26.0 %collective-permute-start = (bf16[64,2]{1,0:T(8,128)(2,1)S(1)}, bf16[64,2]{1,0:T(8,128)(2,1)S(1)}, u32[]{:S(2)}, u32[]{:S(2)}) collective-permute-start(bf16[64,2]{1,0:T(8,128)(2,1)S(1)} %slice.42), channel_id=1, source_target_pairs={{0,16},{16,32},{32,48},{48,64},{64,80},{80,96},{96,112},{112,128},... | collective-permute-start | bytes 776 | tf_op jit(solution)/shard_map/ppermute | solution.py:19
  108.6 11.4 %collective-permute-start.12 = (bf16[1024,128]{1,0:T(8,128)(2,1)S(1)}, bf16[1024,128]{1,0:T(8,128)(2,1)}, u32[]{:S(2)}, u32[]{:S(2)}) collective-permute-start(bf16[1024,128]{1,0:T(8,128)(2,1)S(1)} %collective-permute-done.11), channel_id=1, source_target_pairs={{1,0},{2,1},{3,2},{4,3},{5,4},{6,5},{7,6},{8,7},{9,8},{10,9},{11,1... | collective-permute-start | bytes 786440 | tf_op jit(solution)/shard_map/ppermute | solution.py:104
  115.5 12.0 %collective-permute-start.6 = (bf16[1024,128]{1,0:T(8,128)(2,1)}, bf16[1024,128]{1,0:T(8,128)(2,1)}, u32[]{:S(2)}, u32[]{:S(2)}) collective-permute-start(bf16[1024,128]{1,0:T(8,128)(2,1)} %collective-permute-done.5), channel_id=1, source_target_pairs={{0,1},{1,2},{2,3},{3,4},{4,5},{5,6},{6,7},{7,8},{8,9},{9,10},{10,1... | collective-permute-start | bytes 786440 | tf_op jit(solution)/shard_map/ppermute | solution.py:101
  120.0 11.4 %collective-permute-start.13 = (bf16[1024,128]{1,0:T(8,128)(2,1)}, bf16[1024,128]{1,0:T(8,128)(2,1)}, u32[]{:S(2)}, u32[]{:S(2)}) collective-permute-start(bf16[1024,128]{1,0:T(8,128)(2,1)} %collective-permute-done.12), channel_id=1, source_target_pairs={{1,0},{2,1},{3,2},{4,3},{5,4},{6,5},{7,6},{8,7},{9,8},{10,9},{11,1... | collective-permute-start | bytes 786440 | tf_op jit(solution)/shard_map/ppermute | solution.py:104
  127.5 11.3 %collective-permute-start.7 = (bf16[1024,128]{1,0:T(8,128)(2,1)}, bf16[1024,128]{1,0:T(8,128)(2,1)}, u32[]{:S(2)}, u32[]{:S(2)}) collective-permute-start(bf16[1024,128]{1,0:T(8,128)(2,1)} %collective-permute-done.6), channel_id=1, source_target_pairs={{0,1},{1,2},{2,3},{3,4},{4,5},{5,6},{6,7},{7,8},{8,9},{9,10},{10,1... | collective-permute-start | bytes 786440 | tf_op jit(solution)/shard_map/ppermute | solution.py:101
  131.4 11.4 %collective-permute-start.14 = (bf16[1024,128]{1,0:T(8,128)(2,1)}, bf16[1024,128]{1,0:T(8,128)(2,1)S(1)}, u32[]{:S(2)}, u32[]{:S(2)}) collective-permute-start(bf16[1024,128]{1,0:T(8,128)(2,1)} %collective-permute-done.13), channel_id=1, source_target_pairs={{1,0},{2,1},{3,2},{4,3},{5,4},{6,5},{7,6},{8,7},{9,8},{10,9},{11,1... | collective-permute-start | bytes 786440 | tf_op jit(solution)/shard_map/ppermute | solution.py:104
  138.8 10.9 %collective-permute-start.8 = (bf16[1024,128]{1,0:T(8,128)(2,1)}, bf16[1024,128]{1,0:T(8,128)(2,1)}, u32[]{:S(2)}, u32[]{:S(2)}) collective-permute-start(bf16[1024,128]{1,0:T(8,128)(2,1)} %collective-permute-done.7), channel_id=1, source_target_pairs={{0,1},{1,2},{2,3},{3,4},{4,5},{5,6},{6,7},{7,8},{8,9},{9,10},{10,1... | collective-permute-start | bytes 786440 | tf_op jit(solution)/shard_map/ppermute | solution.py:101
  142.8 23.4 %collective-permute-start.15 = (bf16[1024,128]{1,0:T(8,128)(2,1)S(1)}, bf16[1024,128]{1,0:T(8,128)(2,1)S(1)}, u32[]{:S(2)}, u32[]{:S(2)}) collective-permute-start(bf16[1024,128]{1,0:T(8,128)(2,1)S(1)} %collective-permute-done.14), channel_id=1, source_target_pairs={{1,0},{2,1},{3,2},{4,3},{5,4},{6,5},{7,6},{8,7},{9,8},{10,9},{11,1... | collective-permute-start | bytes 786440 | tf_op jit(solution)/shard_map/ppermute | solution.py:104
  172.3 9.8 %copy-start.3 = (bf16[1,2048,256]{2,1,0:T(8,128)(2,1)S(1)}, bf16[1,2048,256]{2,1,0:T(8,128)(2,1)}, u32[]{:S(2)}) copy-start(bf16[1,2048,256]{2,1,0:T(8,128)(2,1)} %param.19) | copy-start | bytes 3145732
  178.8 3.4 %copy-start.1 = (bf16[1024,16,128]{0,2,1:T(8,128)(2,1)S(1)}, bf16[1024,16,128]{0,2,1:T(8,128)(2,1)}, u32[]{:S(2)}) copy-start(bf16[1024,16,128]{0,2,1:T(8,128)(2,1)} %copy.29) | copy-start | bytes 12582916
  182.2 2.4 copy-start.4
  253.7 18.5 %copy-start.2 = (f32[256,2]{0,1:T(2,128)S(1)}, f32[256,2]{0,1:T(2,128)}, u32[]{:S(2)}) copy-start(f32[256,2]{0,1:T(2,128)} %param.18) | copy-start | bytes 6148
  253.7 18.7 %copy-start.5 = (bf16[1024,128]{1,0:T(8,128)(2,1)S(1)}, bf16[1024,128]{1,0:T(8,128)(2,1)}, u32[]{:S(2)}) copy-start(bf16[1024,128]{1,0:T(8,128)(2,1)} %param.15) | copy-start | bytes 786436
  257.3 37.2 %all-to-all-start.2 = ((bf16[128,32,32]{0,2,1:T(8,128)(2,1)}), bf16[128,32,32]{0,2,1:T(8,128)(2,1)S(1)}, u32[]{:S(2)}, u32[]{:S(2)}) async-start(bf16[128,32,32]{0,2,1:T(8,128)(2,1)} %bitcast.32), calls=%async_computation.2 | async-start | bytes 524288 | tf_op jit(solution)/shard_map/all_to_all | solution.py:122
Sparse Core Ops, SparseCore 0:
  142.9 75.0 all-gather.1
